TPU v7x, 32 devices: a whole 2x2x4 slice. The times are simulated.
32 devices in a mesh: grp: 2 (over y), fs: 4 (over z), tp: 4 (over x, core).
Axes of the slice: x: 2, y: 2, z: 4, core: 2. Of those that a mesh axis runs over, the one named last changes fastest.
Arguments:
- prompt: bfloat16 [8, 1024, 2048], P(('grp', 'tp')), parts along dimension 0, may hold values from -6 to 6
- gate_first: float32 [2048, 5632], P('fs', 'tp'), may hold values from -0.125 to 0.125
- up_first: float32 [2048, 5632], P('fs', 'tp'), may hold values from -0.125 to 0.125
- down_first: float32 [5632, 2048], P('fs', 'tp'), may hold values from -0.3125 to 0.3125
- norm_gain: float32 [2048], replicated, may hold values from 0.1 to 1.9
- gate_second: float32 [2048, 5632], P('fs', 'tp'), may hold values from -0.125 to 0.125
- up_second: float32 [2048, 5632], P('fs', 'tp'), may hold values from -0.125 to 0.125
- down_second: float32 [5632, 2048], P('fs', 'tp'), may hold values from -0.3125 to 0.3125
Outputs:
- result: bfloat16 [8, 1024, 2048], P(('grp', 'tp'), 'fs'), parts along dimension 0
- gate_one: bfloat16 [4096, 5632], P('grp', 'fs'), parts along dimension 0
- up_one: bfloat16 [4096, 5632], P('grp', 'fs'), parts along dimension 0
- down_one: bfloat16 [5632, 4096], P('fs', 'grp'), parts along dimension 1
- gate_two: bfloat16 [4096, 5632], P('grp', 'fs'), parts along dimension 0
- up_two: bfloat16 [4096, 5632], P('grp', 'fs'), parts along dimension 0
- down_two: bfloat16 [5632, 4096], P('fs', 'grp'), parts along dimension 1
There are 2 independent parts, one for each index of `grp`. A program takes and returns all parts, laid end to end along the dimension named above; an argument that names none is the same for every part. Nothing has to cross between parts.
All inputs are finite; a program needn't handle non-finite values.
Results may differ from a plain program's by a relative error of at most 0.029.
Values may be sent and summed in bfloat16 or wider, within the bound.
A program may use at most 192 MiB of HBM per device.

v0:
```python
import jax
import jax.numpy as jnp
from jax import lax
from jax.sharding import PartitionSpec as P

norm_eps = 1e-05
deep_alpha = 2.0**0.25
half_step = 0.5


def plain_norm(values):
    row_mean = jnp.mean(values, axis=-1, keepdims=True)
    centred = values - row_mean
    variance = jnp.mean(centred * centred, axis=-1, keepdims=True)
    return centred * lax.rsqrt(variance + norm_eps)


def gated_hidden(inputs, gate_proj, up_proj):
    gate_act = jnp.dot(inputs, gate_proj, preferred_element_type=jnp.float32)
    up_act = jnp.dot(inputs, up_proj, preferred_element_type=jnp.float32)
    return (jax.nn.silu(gate_act) * up_act).astype(jnp.bfloat16)


def relay_weights(gate_proj, up_proj, down_proj):
    gate_rows, up_rows, down_mine = (
        lax.all_gather(gate_proj, "tp", axis=1, tiled=True),
        lax.all_gather(up_proj, "tp", axis=1, tiled=True),
        lax.all_gather(down_proj, "tp", axis=1, tiled=True),
    )
    gate_mine, up_mine = (
        lax.all_to_all(gate_rows, "fs", split_axis=1, concat_axis=0, tiled=True),
        lax.all_to_all(up_rows, "fs", split_axis=1, concat_axis=0, tiled=True),
    )
    return (gate_mine, up_mine, down_mine)


def row_terms(hidden, down_proj):
    return jnp.dot(hidden, down_proj, preferred_element_type=jnp.float32)


def body(prompt, gate_first, up_first, down_first, norm_gain, gate_second, up_second, down_second):
    fs_index = lax.axis_index("fs")
    row_block = gate_first.shape[0]
    gain_rows = lax.dynamic_slice_in_dim(norm_gain, fs_index * row_block, row_block, 0)
    gate_one, up_one, down_one = relay_weights(
        gate_first.astype(jnp.bfloat16),
        up_first.astype(jnp.bfloat16),
        down_first.astype(jnp.bfloat16),
    )
    gate_two, up_two, down_two = relay_weights(
        (gain_rows[:, None] * gate_second).astype(jnp.bfloat16),
        (gain_rows[:, None] * up_second).astype(jnp.bfloat16),
        down_second.astype(jnp.bfloat16),
    )
    tokens = prompt.reshape(-1, prompt.shape[-1])
    own_count = tokens.shape[0] // lax.axis_size("fs")
    own_first = fs_index * own_count
    hidden_one = gated_hidden(tokens, gate_one, up_one)
    own_tokens = lax.dynamic_slice_in_dim(tokens, own_first, own_count, 0)
    ffn_one = lax.psum_scatter(
        row_terms(hidden_one, down_one).astype(jnp.bfloat16), "fs", scatter_dimension=0, tiled=True
    ).astype(jnp.float32)
    normed_own = plain_norm(
        deep_alpha * own_tokens.astype(jnp.float32) + half_step * ffn_one
    ).astype(jnp.bfloat16)
    hidden_two = gated_hidden(
        lax.all_gather(normed_own, "fs", axis=0, tiled=True), gate_two, up_two
    )
    ffn_two = lax.psum_scatter(
        row_terms(hidden_two, down_two).astype(jnp.bfloat16), "fs", scatter_dimension=0, tiled=True
    ).astype(jnp.float32)
    residual_two = deep_alpha * norm_gain * normed_own.astype(jnp.float32)
    result = plain_norm(residual_two + half_step * ffn_two).astype(jnp.bfloat16)
    return (
        result.reshape(1, result.shape[0], result.shape[-1]),
        gate_one,
        up_one,
        down_one,
        gate_two,
        up_two,
        down_two,
    )


def solution(mesh):
    placed = (
        P(("grp", "tp"), None, None),
        P("fs", "tp"),
        P("fs", "tp"),
        P("fs", "tp"),
        P(),
        P("fs", "tp"),
        P("fs", "tp"),
        P("fs", "tp"),
    )
    return jax.shard_map(
        body,
        mesh=mesh,
        in_specs=placed,
        out_specs=(
            P(("grp", "tp"), "fs", None),
            P("grp", "fs"),
            P("grp", "fs"),
            P("fs", "grp"),
            P("grp", "fs"),
            P("grp", "fs"),
            P("fs", "grp"),
        ),
        check_vma=False,
    )
```

profile of v0, /device:TPU:0, one launch (start us, length us, event | category | flops | bytes accessed | tf_op | source)
XLA Modules:
  0.0 934.5 jit_solution(12915030123418314235)
XLA Ops:
  7.2 3.2 convert_element_type.50
  11.8 44.9 %all-gather.8.cloned.1.call-done = bf16[512,5632]{1,0:T(8,128)(2,1)} async-done(((bf16[512,1408]{1,0:T(8,128)(2,1)}), bf16[512,5632]{1,0:T(8,128)(2,1)}) %all-gather.8.cloned.1.call-update) | async-done | bytes 5767184 | tf_op jit(solution)/shard_map/all_gather | solution.py:26
  56.7 5.6 copy.30
  62.3 5.5 all-to-all-start
  69.2 33.0 %all-gather.10.cloned.1.call-done = bf16[512,5632]{1,0:T(8,128)(2,1)} async-done(((bf16[512,1408]{1,0:T(8,128)(2,1)}), bf16[512,5632]{1,0:T(8,128)(2,1)}) %all-gather.10.cloned.1.call-update) | async-done | bytes 5767184 | tf_op jit(solution)/shard_map/all_gather | solution.py:27
  102.2 5.6 copy.29
  107.8 87.6 %all-to-all-done = bf16[512,4,1408]{2,0,1:T(8,128)(2,1)} async-done(((bf16[512,4,1408]{2,0,1:T(8,128)(2,1)}), bf16[512,4,1408]{2,0,1:T(8,128)(2,1)}, u32[]{:S(2)}, u32[]{:S(2)}) %all-to-all-start) | async-done | bytes 5767200 | tf_op jit(solution)/shard_map/all_to_all | solution.py:31
  195.4 5.5 all-to-all-start.1
  201.1 3.9 multiply_convert_fusion.2
  205.1 11.7 %fusion.1 = f32[1024,1408]{1,0:T(8,128)} fusion(bf16[2048,1408]{1,0:T(8,128)(2,1)} %bitcast.3, bf16[1,1024,2048]{2,1,0:T(8,128)(2,1)} %param.8), kind=kOutput, calls=%fused_computation.7 | convolution fusion | flops 5905580032 | bytes 15728640 | tf_op jit(solution)/shard_map/dot_general | solution.py:19
  216.8 110.9 %all-to-all-done.1 = bf16[512,4,1408]{2,0,1:T(8,128)(2,1)} async-done(((bf16[512,4,1408]{2,0,1:T(8,128)(2,1)}), bf16[512,4,1408]{2,0,1:T(8,128)(2,1)}, u32[]{:S(2)}, u32[]{:S(2)}) %all-to-all-start.1) | async-done | bytes 5767200 | tf_op jit(solution)/shard_map/all_to_all | solution.py:32
  327.7 20.6 %convolution_convert_fusion.1 = bf16[1024,2048]{1,0:T(8,128)(2,1)} fusion(bf16[1408,2048]{1,0:T(8,128)(2,1)} %all-gather.12.cloned.1.call-done, f32[1024,1408]{1,0:T(8,128)} %fusion.1, bf16[2048,1408]{1,0:T(8,128)(2,1)} %bitcast.5, bf16[1,1024,2048]{2,1,0:T(8,128)(2,1)} %param.8), kind=kOutput, calls=%fused_computation.10 | convolution fusion | flops 11821907968 | bytes 25690112 | tf_op jit(solution)/shard_map/dot_general | solution.py:38
  348.9 5.6 copy.28
  354.5 5.2 all-to-all-start.2
  359.7 124.0 %reduce-scatter.3.cloned.1.call-done = bf16[256,2048]{1,0:T(8,128)(2,1)} async-done(((bf16[1024,2048]{1,0:T(8,128)(2,1)}), bf16[256,2048]{1,0:T(8,128)(2,1)}) %reduce-scatter.3.cloned.1.call-update) | async-done | bytes 1048592 | tf_op jit(solution)/shard_map/reduce_scatter | solution.py:60
  483.7 2.1 fusion.4
  485.8 2.2 multiply_reduce_fusion.1
  488.0 2.7 multiply_convert_fusion.5
  492.3 82.7 %all-gather.18.cloned.1.call-done = bf16[512,5632]{1,0:T(8,128)(2,1)} async-done(((bf16[512,1408]{1,0:T(8,128)(2,1)}), bf16[512,5632]{1,0:T(8,128)(2,1)}) %all-gather.18.cloned.1.call-update) | async-done | bytes 5767184 | tf_op jit(solution)/shard_map/all_gather | solution.py:27
  575.0 5.6 copy.27
  580.6 5.3 all-to-all-start.3
  585.9 167.0 %all-gather.14.cloned.1.call-done = bf16[1024,2048]{1,0:T(8,128)(2,1)} async-done(((bf16[256,2048]{1,0:T(8,128)(2,1)}), bf16[1024,2048]{1,0:T(8,128)(2,1)}) %all-gather.14.cloned.1.call-update) | async-done | bytes 4194320 | tf_op jit(solution)/shard_map/all_gather | solution.py:67
  753.0 11.7 %fusion.6 = f32[1024,1408]{1,0:T(8,128)} fusion(bf16[1024,2048]{1,0:T(8,128)(2,1)} %all-gather.14.cloned.1.call-done, bf16[2048,1408]{1,0:T(8,128)(2,1)} %bitcast.7), kind=kOutput, calls=%fused_computation.27 | convolution fusion | flops 5905580032 | bytes 15728640 | tf_op jit(solution)/shard_map/dot_general | solution.py:19
  764.7 32.5 %all-gather.20.cloned.1.call-done = bf16[1408,2048]{1,0:T(8,128)(2,1)} async-done(((bf16[1408,512]{1,0:T(8,128)(2,1)}), bf16[1408,2048]{1,0:T(8,128)(2,1)}) %all-gather.20.cloned.1.call-update) | async-done | bytes 5767184 | tf_op jit(solution)/shard_map/all_gather | solution.py:28
  797.2 20.6 %convolution_convert_fusion = bf16[1024,2048]{1,0:T(8,128)(2,1)} fusion(bf16[1408,2048]{1,0:T(8,128)(2,1)} %all-gather.20.cloned.1.call-done, f32[1024,1408]{1,0:T(8,128)} %fusion.6, bf16[1024,2048]{1,0:T(8,128)(2,1)} %all-gather.14.cloned.1.call-done, bf16[2048,1408]{1,0:T(8,128)(2,1)} %bitcast.9), kind=kOutput, calls=%fused_computation.9 | convolution fusion | flops 11821907968 | bytes 25690112 | tf_op jit(solution)/shard_map/dot_general | solution.py:38
  817.8 76.9 %reduce-scatter.5.cloned.1.call-done = bf16[256,2048]{1,0:T(8,128)(2,1)} async-done(((bf16[1024,2048]{1,0:T(8,128)(2,1)}), bf16[256,2048]{1,0:T(8,128)(2,1)}) %reduce-scatter.5.cloned.1.call-update) | async-done | bytes 1048592 | tf_op jit(solution)/shard_map/reduce_scatter | solution.py:69
  900.1 5.7 copy.37
  905.8 5.6 copy.38
  911.4 2.5 copy.39
  914.0 5.7 copy.40
  919.7 5.7 copy.41
  925.4 2.5 copy.42
  (60 shorter events, 10.5 us)
Async XLA Ops:
  7.2 3.3 copy-start.4
  7.2 49.5 %all-gather.8.cloned.1.call-start = ((), (), s32[]{:S(2)}) async-start(), calls=%async_computation.6 | async-start | bytes 7208960 | tf_op jit(solution)/shard_map/all_gather | solution.py:26
  10.5 91.8 %all-gather.10.cloned.1.call-start = ((), (), s32[]{:S(2)}) async-start(), calls=%async_computation.7 | async-start | bytes 7208960 | tf_op jit(solution)/shard_map/all_gather | solution.py:27
  62.3 5.6 copy-start.5
  62.3 133.1 %all-to-all-start = ((bf16[512,4,1408]{2,0,1:T(8,128)(2,1)}), bf16[512,4,1408]{2,0,1:T(8,128)(2,1)}, u32[]{:S(2)}, u32[]{:S(2)}) async-start(bf16[512,4,1408]{2,0,1:T(8,128)(2,1)} %bitcast.71), calls=%async_computation | async-start | bytes 11534336 | tf_op jit(solution)/shard_map/all_to_all | solution.py:31
  67.8 148.9 %all-gather.12.cloned.1.call-start = ((), (), s32[]{:S(2)}) async-start(), calls=%async_computation.8 | async-start | bytes 7208960 | tf_op jit(solution)/shard_map/all_gather | solution.py:28
  195.4 5.5 copy-start.7
  195.4 5.6 copy-start.3
  195.4 132.2 %all-to-all-start.1 = ((bf16[512,4,1408]{2,0,1:T(8,128)(2,1)}), bf16[512,4,1408]{2,0,1:T(8,128)(2,1)}, u32[]{:S(2)}, u32[]{:S(2)}) async-start(bf16[512,4,1408]{2,0,1:T(8,128)(2,1)} %bitcast.70), calls=%async_computation.1 | async-start | bytes 11534336 | tf_op jit(solution)/shard_map/all_to_all | solution.py:32
  200.9 147.9 %all-gather.16.cloned.1.call-start = ((), (), s32[]{:S(2)}) async-start(), calls=%async_computation.11 | async-start | bytes 7208960 | tf_op jit(solution)/shard_map/all_gather | solution.py:26
  205.0 278.6 %reduce-scatter.3.cloned.1.call-start = ((), (), s32[]{:S(2)}) async-start(), calls=%async_computation.9 | async-start | bytes 5242880 | tf_op jit(solution)/shard_map/reduce_scatter | solution.py:60
  348.2 226.7 %all-gather.18.cloned.1.call-start = ((), (), s32[]{:S(2)}) async-start(), calls=%async_computation.12 | async-start | bytes 7208960 | tf_op jit(solution)/shard_map/all_gather | solution.py:27
  354.5 226.1 %all-to-all-start.2 = ((bf16[512,4,1408]{2,0,1:T(8,128)(2,1)}), bf16[512,4,1408]{2,0,1:T(8,128)(2,1)}, u32[]{:S(2)}, u32[]{:S(2)}) async-start(bf16[512,4,1408]{2,0,1:T(8,128)(2,1)} %bitcast.69), calls=%async_computation.3 | async-start | bytes 11534336 | tf_op jit(solution)/shard_map/all_to_all | solution.py:31
  359.6 393.4 %all-gather.14.cloned.1.call-start = ((), (), s32[]{:S(2)}) async-start(), calls=%async_computation.10 | async-start | bytes 5242880 | tf_op jit(solution)/shard_map/all_gather | solution.py:67
  359.7 131.3 %copy-start.6 = (f32[1408,512]{1,0:T(8,128)S(1)}, f32[1408,512]{1,0:T(8,128)}, u32[]{:S(2)}) copy-start(f32[1408,512]{1,0:T(8,128)} %param.15) | copy-start | bytes 8650756
  483.7 4.3 copy-start.1
  490.8 306.4 %all-gather.20.cloned.1.call-start = ((), (), s32[]{:S(2)}) async-start(), calls=%async_computation.13 | async-start | bytes 7208960 | tf_op jit(solution)/shard_map/all_gather | solution.py:28
  580.6 216.6 %all-to-all-start.3 = ((bf16[512,4,1408]{2,0,1:T(8,128)(2,1)}), bf16[512,4,1408]{2,0,1:T(8,128)(2,1)}, u32[]{:S(2)}, u32[]{:S(2)}) async-start(bf16[512,4,1408]{2,0,1:T(8,128)(2,1)} %bitcast.72), calls=%async_computation.4 | async-start | bytes 11534336 | tf_op jit(solution)/shard_map/all_to_all | solution.py:32
  585.9 308.8 %reduce-scatter.5.cloned.1.call-start = ((), (), s32[]{:S(2)}) async-start(), calls=%async_computation.14 | async-start | bytes 5242880 | tf_op jit(solution)/shard_map/reduce_scatter | solution.py:69
  817.8 77.0 %copy-start = (bf16[256,2048]{1,0:T(8,128)(2,1)S(1)}, bf16[256,2048]{1,0:T(8,128)(2,1)}, u32[]{:S(2)}) copy-start(bf16[256,2048]{1,0:T(8,128)(2,1)} %multiply_convert_fusion.5) | copy-start | bytes 3145732
  894.7 3.8 copy-start.2
  896.6 14.9 %slice-start = ((s8[5767168]{0:T(1024)(128)(4,1)}), s8[4194304]{0:T(1024)(128)(4,1)S(1)}, s32[]{:S(2)}) async-start(s8[5767168]{0:T(1024)(128)(4,1)} %bitcast.73), calls=%async_computation.15 | async-start | bytes 8388608
  900.1 11.3 %slice-start.1 = ((s8[5767168]{0:T(1024)(128)(4,1)}), s8[1572864]{0:T(1024)(128)(4,1)S(1)}, s32[]{:S(2)}) async-start(s8[5767168]{0:T(1024)(128)(4,1)} %bitcast.73), calls=%async_computation.16 | async-start | bytes 3145728
  913.9 11.5 %slice-start.2 = ((s8[5767168]{0:T(1024)(128)(4,1)}), s8[4194304]{0:T(1024)(128)(4,1)S(1)}, s32[]{:S(2)}) async-start(s8[5767168]{0:T(1024)(128)(4,1)} %bitcast.75), calls=%async_computation.17 | async-start | bytes 8388608
  919.7 5.7 slice-start.3
Sparse Core Ops, SparseCore 0:
  10.6 46.0 all-gather.7
  58.8 43.3 all-gather.9
  104.4 43.3 all-gather.11
  205.2 43.7 all-gather.15
  348.4 135.2 reduce-scatter.2
  485.7 89.2 all-gather.17
  577.1 175.8 all-gather.13
  755.1 42.0 all-gather.19
  817.9 76.7 reduce-scatter.4
where the time goes:
time: 935 us; the launch traced here: 934 us
  waiting for transfers between devices  760 us (81%)
  matrix products  64.5 us (7%)
  local copies, waits for them, and re-layouts  50.3 us (5%)
  other arithmetic  23.4 us (3%)
  starting transfers between devices  22.1 us (2%)
  between operations  14 us (1%)
    all_gather x1, waiting for transfers between devices, body(): lax.all_gather(normed_own, 'fs', axis=0, tiled=True)  167 us
    reduce_scatter x1, waiting for transfers between devices, body(): lax.psum_scatter(row_terms(hidden_one, down_one).astype(jnp.bfloat16), 'f...  124 us
    all_gather x2, waiting for transfers between devices, relay_weights(): lax.all_gather(up_proj, 'tp', axis=1, tiled=True)  116 us
    all_to_all x2, waiting for transfers between devices, relay_weights(): lax.all_to_all(up_rows, 'fs', split_axis=1, concat_axis=0, tiled=True)  111 us
    all_to_all x2, waiting for transfers between devices, relay_weights(): lax.all_to_all(gate_rows, 'fs', split_axis=1, concat_axis=0, tiled=True)  87.6 us
    reduce_scatter x1, waiting for transfers between devices, body(): lax.psum_scatter(row_terms(hidden_two, down_two).astype(jnp.bfloat16), 'f...  76.9 us
    all_gather x2, waiting for transfers between devices, relay_weights(): lax.all_gather(gate_proj, 'tp', axis=1, tiled=True)  44.9 us
    dot_general x2, matrix products, row_terms(): return jnp.dot(hidden, down_proj, preferred_element_type=jnp.float32)  41.1 us
  transfers between devices with their start and end apart: 13, of which 9 were waited for; matrix products, arithmetic and copies ran while one was open for 9% of the time, Pallas kernels for 0%

commit v1 on v0

--- a/solution.py
+++ b/solution.py
@@ -24,7 +24,7 @@
 def relay_weights(gate_proj, up_proj, down_proj):
     gate_rows, up_rows, down_mine = (
         lax.all_gather(gate_proj, "tp", axis=1, tiled=True),
-        lax.all_gather(up_proj, "tp", axis=1, tiled=True),
+        jnp.concatenate(lax.all_gather(up_proj, "tp"), axis=1),
         lax.all_gather(down_proj, "tp", axis=1, tiled=True),
     )
     gate_mine, up_mine = (

time: 935 us -> 935 us (level)
  waiting for transfers between devices: 760 us -> 772 us
  local copies, waits for them, and re-layouts: 50.3 us -> 39.3 us
    all_to_all x2 -> x0, local copies, waits for them, and re-layouts: 11.2 us -> none  [relay_weights(): lax.all_to_all(up_rows, 'fs', split_axis=1, concat_axis=0, tiled=True)]
  transfers between devices with their start and end apart: 13 -> 13, of which waited for: 9 -> 9; matrix products, arithmetic and copies ran while one was open for 9% -> 7% of each run, Pallas kernels for 0% -> 0%
where the time goes in v1:
time: 935 us; the launch traced here: 934 us
  waiting for transfers between devices  772 us (83%)
  matrix products  64.5 us (7%)
  local copies, waits for them, and re-layouts  39.3 us (4%)
  other arithmetic  23.2 us (2%)
  starting transfers between devices  21.9 us (2%)
  between operations  14 us (1%)
    all_gather x1, waiting for transfers between devices, body(): lax.all_gather(normed_own, 'fs', axis=0, tiled=True)  168 us
    reduce_scatter x1, waiting for transfers between devices, body(): lax.psum_scatter(row_terms(hidden_one, down_one).astype(jnp.bfloat16), 'f...  124 us
    all_gather x2, waiting for transfers between devices, relay_weights(): lax.all_gather(up_proj, 'tp')  116 us
    all_to_all x2, waiting for transfers between devices, relay_weights(): lax.all_to_all(up_rows, 'fs', split_axis=1, concat_axis=0, tiled=True)  111 us
    all_to_all x2, waiting for transfers between devices, relay_weights(): lax.all_to_all(gate_rows, 'fs', split_axis=1, concat_axis=0, tiled=True)  93.2 us
    reduce_scatter x1, waiting for transfers between devices, body(): lax.psum_scatter(row_terms(hidden_two, down_two).astype(jnp.bfloat16), 'f...  76.9 us
    all_gather x2, waiting for transfers between devices, relay_weights(): lax.all_gather(gate_proj, 'tp', axis=1, tiled=True)  44.9 us
    dot_general x2, matrix products, row_terms(): return jnp.dot(hidden, down_proj, preferred_element_type=jnp.float32)  41.1 us
  transfers between devices with their start and end apart: 13, of which 9 were waited for; matrix products, arithmetic and copies ran while one was open for 7% of the time, Pallas kernels for 0%

profile of v1, /device:TPU:0, one launch (start us, length us, event | category | flops | bytes accessed | tf_op | source)
XLA Modules:
  0.0 934.5 jit_solution(7914213906517003144)
XLA Ops:
  7.2 3.2 convert_element_type.50
  11.8 44.9 %all-gather.10.cloned.1.call-done = bf16[512,5632]{1,0:T(8,128)(2,1)} async-done(((bf16[512,1408]{1,0:T(8,128)(2,1)}), bf16[512,5632]{1,0:T(8,128)(2,1)}) %all-gather.10.cloned.1.call-update) | async-done | bytes 5767184 | tf_op jit(solution)/shard_map/all_gather | solution.py:26
  56.7 5.6 copy.22
  62.3 5.5 all-to-all-start
  69.2 33.0 %all-gather.20.cloned.1.call-done = bf16[2048,1408]{1,0:T(8,128)(2,1)} async-done(((bf16[512,1408]{1,0:T(8,128)(2,1)}), bf16[2048,1408]{1,0:T(8,128)(2,1)}) %all-gather.20.cloned.1.call-update) | async-done | bytes 5767184 | tf_op jit(solution)/shard_map/all_gather | solution.py:27
  102.2 93.2 %all-to-all-done = bf16[512,4,1408]{2,0,1:T(8,128)(2,1)} async-done(((bf16[512,4,1408]{2,0,1:T(8,128)(2,1)}), bf16[512,4,1408]{2,0,1:T(8,128)(2,1)}, u32[]{:S(2)}, u32[]{:S(2)}) %all-to-all-start) | async-done | bytes 5767200 | tf_op jit(solution)/shard_map/all_to_all | solution.py:31
  195.4 5.5 all-to-all-start.1
  201.1 3.9 multiply_convert_fusion.2
  205.1 11.7 %fusion.1 = f32[1024,1408]{1,0:T(8,128)} fusion(bf16[2048,1408]{1,0:T(8,128)(2,1)} %bitcast.3, bf16[1,1024,2048]{2,1,0:T(8,128)(2,1)} %param.8), kind=kOutput, calls=%fused_computation.5 | convolution fusion | flops 5905580032 | bytes 15728640 | tf_op jit(solution)/shard_map/dot_general | solution.py:19
  216.8 110.9 %all-to-all-done.1 = bf16[512,4,1408]{2,0,1:T(8,128)(2,1)} async-done(((bf16[512,4,1408]{2,0,1:T(8,128)(2,1)}), bf16[512,4,1408]{2,0,1:T(8,128)(2,1)}, u32[]{:S(2)}, u32[]{:S(2)}) %all-to-all-start.1) | async-done | bytes 5767200 | tf_op jit(solution)/shard_map/all_to_all | solution.py:32
  327.7 20.6 %convolution_convert_fusion.1 = bf16[1024,2048]{1,0:T(8,128)(2,1)} fusion(bf16[1408,2048]{1,0:T(8,128)(2,1)} %all-gather.12.cloned.1.call-done, f32[1024,1408]{1,0:T(8,128)} %fusion.1, bf16[2048,1408]{1,0:T(8,128)(2,1)} %bitcast.7, bf16[1,1024,2048]{2,1,0:T(8,128)(2,1)} %param.8), kind=kOutput, calls=%fused_computation.8 | convolution fusion | flops 11821907968 | bytes 25690112 | tf_op jit(solution)/shard_map/dot_general | solution.py:38
  348.9 5.6 copy.21
  354.5 5.2 all-to-all-start.2
  359.7 124.0 %reduce-scatter.3.cloned.1.call-done = bf16[256,2048]{1,0:T(8,128)(2,1)} async-done(((bf16[1024,2048]{1,0:T(8,128)(2,1)}), bf16[256,2048]{1,0:T(8,128)(2,1)}) %reduce-scatter.3.cloned.1.call-update) | async-done | bytes 1048592 | tf_op jit(solution)/shard_map/reduce_scatter | solution.py:60
  483.7 2.1 fusion.4
  485.8 2.2 multiply_reduce_fusion.1
  488.0 2.7 multiply_convert_fusion.5
  492.1 82.8 %all-gather.22.cloned.1.call-done = bf16[2048,1408]{1,0:T(8,128)(2,1)} async-done(((bf16[512,1408]{1,0:T(8,128)(2,1)}), bf16[2048,1408]{1,0:T(8,128)(2,1)}) %all-gather.22.cloned.1.call-update) | async-done | bytes 5767184 | tf_op jit(solution)/shard_map/all_gather | solution.py:27
  575.0 5.2 all-to-all-start.3
  580.4 167.9 %all-gather.14.cloned.1.call-done = bf16[1024,2048]{1,0:T(8,128)(2,1)} async-done(((bf16[256,2048]{1,0:T(8,128)(2,1)}), bf16[1024,2048]{1,0:T(8,128)(2,1)}) %all-gather.14.cloned.1.call-update) | async-done | bytes 4194320 | tf_op jit(solution)/shard_map/all_gather | solution.py:67
  748.3 11.7 %fusion.6 = f32[1024,1408]{1,0:T(8,128)} fusion(bf16[1024,2048]{1,0:T(8,128)(2,1)} %all-gather.14.cloned.1.call-done, bf16[2048,1408]{1,0:T(8,128)(2,1)} %bitcast.9), kind=kOutput, calls=%fused_computation.25 | convolution fusion | flops 5905580032 | bytes 15728640 | tf_op jit(solution)/shard_map/dot_general | solution.py:19
  760.0 37.2 %all-gather.18.cloned.1.call-done = bf16[1408,2048]{1,0:T(8,128)(2,1)} async-done(((bf16[1408,512]{1,0:T(8,128)(2,1)}), bf16[1408,2048]{1,0:T(8,128)(2,1)}) %all-gather.18.cloned.1.call-update) | async-done | bytes 5767184 | tf_op jit(solution)/shard_map/all_gather | solution.py:28
  797.2 20.6 %convolution_convert_fusion = bf16[1024,2048]{1,0:T(8,128)(2,1)} fusion(bf16[1408,2048]{1,0:T(8,128)(2,1)} %all-gather.18.cloned.1.call-done, f32[1024,1408]{1,0:T(8,128)} %fusion.6, bf16[1024,2048]{1,0:T(8,128)(2,1)} %all-gather.14.cloned.1.call-done, bf16[2048,1408]{1,0:T(8,128)(2,1)} %bitcast.13), kind=kOutput, calls=%fused_computation.7 | convolution fusion | flops 11821907968 | bytes 25690112 | tf_op jit(solution)/shard_map/dot_general | solution.py:38
  817.8 76.9 %reduce-scatter.5.cloned.1.call-done = bf16[256,2048]{1,0:T(8,128)(2,1)} async-done(((bf16[1024,2048]{1,0:T(8,128)(2,1)}), bf16[256,2048]{1,0:T(8,128)(2,1)}) %reduce-scatter.5.cloned.1.call-update) | async-done | bytes 1048592 | tf_op jit(solution)/shard_map/reduce_scatter | solution.py:69
  894.7 1.8 fusion.3
  896.6 1.9 multiply_reduce_fusion
  899.9 5.7 copy.29
  905.7 5.7 copy.30
  911.4 2.5 copy.31
  913.9 5.7 copy.32
  919.7 5.7 copy.33
  925.4 2.5 copy.34
  (58 shorter events, 6.7 us)
Async XLA Ops:
  7.2 3.3 copy-start.4
  7.2 49.5 %all-gather.10.cloned.1.call-start = ((), (), s32[]{:S(2)}) async-start(), calls=%async_computation.6 | async-start | bytes 7208960 | tf_op jit(solution)/shard_map/all_gather | solution.py:26
  10.5 91.8 %all-gather.20.cloned.1.call-start = ((), (), s32[]{:S(2)}) async-start(), calls=%async_computation.13 | async-start | bytes 7208960 | tf_op jit(solution)/shard_map/all_gather | solution.py:27
  62.3 5.6 copy-start.5
  62.3 133.1 %all-to-all-start = ((bf16[512,4,1408]{2,0,1:T(8,128)(2,1)}), bf16[512,4,1408]{2,0,1:T(8,128)(2,1)}, u32[]{:S(2)}, u32[]{:S(2)}) async-start(bf16[512,4,1408]{2,0,1:T(8,128)(2,1)} %bitcast.68), calls=%async_computation | async-start | bytes 11534336 | tf_op jit(solution)/shard_map/all_to_all | solution.py:31
  67.9 148.9 %all-gather.12.cloned.1.call-start = ((), (), s32[]{:S(2)}) async-start(), calls=%async_computation.7 | async-start | bytes 7208960 | tf_op jit(solution)/shard_map/all_gather | solution.py:28
  195.4 5.5 copy-start.7
  195.4 5.6 copy-start.3
  195.4 132.2 %all-to-all-start.1 = ((bf16[512,4,1408]{2,0,1:T(8,128)(2,1)}), bf16[512,4,1408]{2,0,1:T(8,128)(2,1)}, u32[]{:S(2)}, u32[]{:S(2)}) async-start(bf16[512,4,1408]{2,0,1:T(8,128)(2,1)} %bitcast.72), calls=%async_computation.1 | async-start | bytes 11534336 | tf_op jit(solution)/shard_map/all_to_all | solution.py:32
  200.9 147.9 %all-gather.16.cloned.1.call-start = ((), (), s32[]{:S(2)}) async-start(), calls=%async_computation.10 | async-start | bytes 7208960 | tf_op jit(solution)/shard_map/all_gather | solution.py:26
  205.0 278.6 %reduce-scatter.3.cloned.1.call-start = ((), (), s32[]{:S(2)}) async-start(), calls=%async_computation.8 | async-start | bytes 5242880 | tf_op jit(solution)/shard_map/reduce_scatter | solution.py:60
  348.2 226.7 %all-gather.22.cloned.1.call-start = ((), (), s32[]{:S(2)}) async-start(), calls=%async_computation.14 | async-start | bytes 7208960 | tf_op jit(solution)/shard_map/all_gather | solution.py:27
  354.5 220.5 %all-to-all-start.2 = ((bf16[512,4,1408]{2,0,1:T(8,128)(2,1)}), bf16[512,4,1408]{2,0,1:T(8,128)(2,1)}, u32[]{:S(2)}, u32[]{:S(2)}) async-start(bf16[512,4,1408]{2,0,1:T(8,128)(2,1)} %bitcast.67), calls=%async_computation.3 | async-start | bytes 11534336 | tf_op jit(solution)/shard_map/all_to_all | solution.py:31
  359.6 388.7 %all-gather.14.cloned.1.call-start = ((), (), s32[]{:S(2)}) async-start(), calls=%async_computation.9 | async-start | bytes 5242880 | tf_op jit(solution)/shard_map/all_gather | solution.py:67
  359.7 131.1 %copy-start.6 = (f32[1408,512]{1,0:T(8,128)S(1)}, f32[1408,512]{1,0:T(8,128)}, u32[]{:S(2)}) copy-start(f32[1408,512]{1,0:T(8,128)} %param.15) | copy-start | bytes 8650756
  483.7 4.3 copy-start.1
  490.7 306.5 %all-gather.18.cloned.1.call-start = ((), (), s32[]{:S(2)}) async-start(), calls=%async_computation.11 | async-start | bytes 7208960 | tf_op jit(solution)/shard_map/all_gather | solution.py:28
  575.0 222.2 %all-to-all-start.3 = ((bf16[512,4,1408]{2,0,1:T(8,128)(2,1)}), bf16[512,4,1408]{2,0,1:T(8,128)(2,1)}, u32[]{:S(2)}, u32[]{:S(2)}) async-start(bf16[512,4,1408]{2,0,1:T(8,128)(2,1)} %bitcast.71), calls=%async_computation.4 | async-start | bytes 11534336 | tf_op jit(solution)/shard_map/all_to_all | solution.py:32
  580.2 314.6 %reduce-scatter.5.cloned.1.call-start = ((), (), s32[]{:S(2)}) async-start(), calls=%async_computation.12 | async-start | bytes 5242880 | tf_op jit(solution)/shard_map/reduce_scatter | solution.py:69
  817.8 77.0 %copy-start = (bf16[256,2048]{1,0:T(8,128)(2,1)S(1)}, bf16[256,2048]{1,0:T(8,128)(2,1)}, u32[]{:S(2)}) copy-start(bf16[256,2048]{1,0:T(8,128)(2,1)} %multiply_convert_fusion.5) | copy-start | bytes 3145732
  894.7 3.7 copy-start.2
  899.9 11.5 %slice-start = ((s8[5767168]{0:T(1024)(128)(4,1)}), s8[4194304]{0:T(1024)(128)(4,1)S(1)}, s32[]{:S(2)}) async-start(s8[5767168]{0:T(1024)(128)(4,1)} %bitcast.69), calls=%async_computation.15 | async-start | bytes 8388608
  905.7 5.7 slice-start.1
  913.9 11.5 %slice-start.2 = ((s8[5767168]{0:T(1024)(128)(4,1)}), s8[4194304]{0:T(1024)(128)(4,1)S(1)}, s32[]{:S(2)}) async-start(s8[5767168]{0:T(1024)(128)(4,1)} %bitcast.73), calls=%async_computation.17 | async-start | bytes 8388608
  919.7 5.7 slice-start.3
Sparse Core Ops, SparseCore 0:
  10.6 46.0 all-gather.9
  58.8 43.3 all-gather.19
  104.4 43.3 all-gather.11
  205.2 43.7 all-gather.15
  348.4 135.2 reduce-scatter.2
  485.7 89.2 all-gather.21
  577.1 171.1 all-gather.13
  750.4 46.6 all-gather.17
  817.9 76.7 reduce-scatter.4
